TPU v7x, 32 devices: a whole 2x2x4 slice. The times are simulated.
32 devices in a mesh: grp: 2 (over x), ep: 16 (over z, y, core).
Axes of the slice: x: 2, y: 2, z: 4, core: 2. Of those that a mesh axis runs over, the one named last changes fastest.
Arguments:
- tokens: bfloat16 [8192, 2048], P(('grp', 'ep')), parts along dimension 0, may hold values from -6 to 6
- norm_gain: float32 [2048], replicated, may hold values from 0.1 to 1.9
- expert_ids: int32 [8192, 2], P(('grp', 'ep')), parts along dimension 0, may hold values from 0 to 15, all different within a row; in each aligned block of 256 rows (0 to 255, 256 to 511, ...) at most 64 rows name the same one
- gate_weights: float32 [8192, 2], P(('grp', 'ep')), parts along dimension 0, may hold values from 0.1 to 1
- w_gate: bfloat16 [16, 2048, 1024], P('ep'), may hold values from -0.125 to 0.125
- w_up: bfloat16 [16, 2048, 1024], P('ep'), may hold values from -0.125 to 0.125
- w_down: bfloat16 [16, 1024, 2048], P('ep'), may hold values from -0.1875 to 0.1875
Outputs:
- mixed: bfloat16 [8192, 2048], P(('grp', 'ep')), parts along dimension 0
There are 2 independent parts, one for each index of `grp`. A program takes and returns all parts, laid end to end along the dimension named above; an argument that names none is the same for every part. Nothing has to cross between parts.
Inputs may be any that keep to these rules, and one draw needn't show every extreme that they name: `expert_ids`: A token's 2 experts are distinct. Within the rows of one device (aligned blocks of 256 tokens) no expert is named more than 64 times, and in some block one expert is named exactly 64 times.
All inputs are finite; a program needn't handle non-finite values.
Results may differ from a plain program's by a relative error of at most 0.0071.
Values may be sent and summed in bfloat16 or wider, within the bound.
A program may use at most 64 MiB of HBM per device.

v0:
```python
import jax
import jax.numpy as jnp
from jax import lax
from jax.sharding import PartitionSpec as P


def per_device(tokens, norm_gain, expert_ids, gate_weights, w_gate, w_up, w_down):
    experts = lax.axis_size("ep")
    tok_rows, feature_width = tokens.shape
    top_count = expert_ids.shape[1]
    capacity = 2 * tok_rows * top_count // experts
    values = tokens.astype(jnp.float32)
    normed = (
        values * lax.rsqrt(jnp.mean(values * values, -1, keepdims=True) + 1e-06) * norm_gain
    ).astype(jnp.bfloat16)
    flat_ids = expert_ids.reshape(-1)
    onehot = (flat_ids[:, None] == jnp.arange(experts, dtype=jnp.int32)[None, :]).astype(jnp.int32)
    before = jnp.cumsum(onehot, axis=0) - onehot
    slots = jnp.sum(onehot * before, axis=1)
    dest = flat_ids * capacity + slots
    copies = jnp.repeat(normed, top_count, axis=0)
    outgoing = jnp.zeros((experts * capacity, feature_width), jnp.bfloat16).at[dest].set(copies)
    outgoing = outgoing.reshape(experts, capacity, feature_width)
    arrived = lax.all_to_all(outgoing, "ep", split_axis=0, concat_axis=0, tiled=True)
    rows = arrived.reshape(-1, feature_width)
    gate = jnp.dot(rows, w_gate[0], preferred_element_type=jnp.float32)
    upper = jnp.dot(rows, w_up[0], preferred_element_type=jnp.float32)
    hidden = (jax.nn.silu(gate) * upper).astype(jnp.bfloat16)
    result = jnp.dot(hidden, w_down[0], preferred_element_type=jnp.float32).astype(jnp.bfloat16)
    finished = result.reshape(arrived.shape)
    returned = lax.all_to_all(finished, "ep", split_axis=0, concat_axis=0, tiled=True)
    returned = returned.reshape(experts * capacity, feature_width)
    back = returned[dest].astype(jnp.float32).reshape(tok_rows, top_count, feature_width)
    mixed = jnp.sum(back * gate_weights[:, :, None], axis=1)
    return mixed.astype(jnp.bfloat16)


def solution(mesh):
    return jax.shard_map(
        per_device,
        mesh=mesh,
        in_specs=(
            P(("grp", "ep"), None),
            P(),
            P(("grp", "ep"), None),
            P(("grp", "ep"), None),
            P("ep", None, None),
            P("ep", None, None),
            P("ep", None, None),
        ),
        out_specs=P(("grp", "ep"), None),
        check_vma=False,
    )
```

profile of v0, /device:TPU:15, one launch (start us, length us, event | category | flops | bytes accessed | tf_op | source)
XLA Modules:
  0.0 251.3 jit_solution(1412394501505923873)
XLA Ops:
  0.0 0.8 copy.10
  0.8 0.1 eq.29
  1.0 0.1 eq.25
  1.1 0.7 broadcast_multiply_fusion
  1.8 1.1 reduce-window.6
  2.9 0.2 slice_reduce_fusion
  3.2 0.1 copy.9
  3.4 0.1 mul.55
  3.5 1.5 fusion.11
  5.0 1.5 fusion.13
  6.6 1.3 broadcast_in_dim.5
  7.8 2.2 reshape.94
  10.1 0.1 fusion.18
  10.2 7.2 %scatter_custom_fusion = bf16[1024,2048]{1,0:T(8,128)(2,1)} fusion(s32[512]{0:T(512)S(1)} %bitcast.45, bf16[512,2048]{1,0:T(8,128)(2,1)} %reshape.94, bf16[]{:T(256)} %constant.8.clone.1), kind=kCustom, calls=%fused_computation.16 | custom fusion | bytes 4194816 | tf_op jit(solution)/shard_map/scatter | solution.py:22
  17.4 99.0 %all_to_all.10 = bf16[16,64,2048]{2,1,0:T(8,128)(2,1)S(1)} all-to-all(bf16[16,64,2048]{2,1,0:T(8,128)(2,1)} %bitcast.41), channel_id=1, replica_groups=mesh['grp'=2,'ep'=16] {'ep'}, dimensions={0} | all-to-all | bytes 8388608 | tf_op jit(solution)/shard_map/all_to_all | solution.py:24
  116.4 4.5 %fusion.2 = f32[1024,1024]{1,0:T(8,128)S(1)} fusion(bf16[1024,2048]{1,0:T(8,128)(2,1)S(1)} %bitcast.43, bf16[1,2048,1024]{2,1,0:T(8,128)(2,1)S(1)} %copy-done.1), kind=kOutput, calls=%fused_computation.4 | convolution fusion | flops 4294967296 | bytes 12582912 | tf_op jit(solution)/shard_map/dot_general | solution.py:27
  121.0 5.4 %multiply_convert_fusion = bf16[1024,1024]{1,0:T(8,128)(2,1)S(1)} fusion(f32[1024,1024]{1,0:T(8,128)S(1)} %fusion.2, bf16[1024,2048]{1,0:T(8,128)(2,1)S(1)} %bitcast.44, bf16[1,2048,1024]{2,1,0:T(8,128)(2,1)S(1)} %copy-done.2), kind=kOutput, calls=%fused_computation.9 | convolution fusion | flops 4301258752 | bytes 14680064 | tf_op jit(solution)/shard_map/dot_general | solution.py:26
  126.3 6.1 %fusion.6 = bf16[1024,2048]{1,0:T(8,128)(2,1)} fusion(bf16[1024,1024]{1,0:T(8,128)(2,1)S(1)} %multiply_convert_fusion, bf16[1,1024,2048]{2,1,0:T(8,128)(2,1)S(1)} %copy-done.3), kind=kOutput, calls=%fused_computation.10 | convolution fusion | flops 4297064448 | bytes 10485760 | tf_op jit(solution)/shard_map/dot_general | solution.py:29
  132.4 5.3 %all-to-all-start.1 = ((bf16[16,64,2048]{2,1,0:T(8,128)(2,1)}), bf16[16,64,2048]{2,1,0:T(8,128)(2,1)}, u32[]{:S(2)}, u32[]{:S(2)}) async-start(bf16[16,64,2048]{2,1,0:T(8,128)(2,1)} %bitcast.42), calls=%async_computation.1 | async-start | bytes 8388608 | tf_op jit(solution)/shard_map/all_to_all | solution.py:31
  137.8 0.1 copy.13
  137.9 92.3 %all-to-all-done.1 = bf16[16,64,2048]{2,1,0:T(8,128)(2,1)} async-done(((bf16[16,64,2048]{2,1,0:T(8,128)(2,1)}), bf16[16,64,2048]{2,1,0:T(8,128)(2,1)}, u32[]{:S(2)}, u32[]{:S(2)}) %all-to-all-start.1) | async-done | bytes 4194336 | tf_op jit(solution)/shard_map/all_to_all | solution.py:31
  230.2 7.1 %gather_fusion = bf16[512,2048]{1,0:T(8,128)(2,1)S(1)} fusion(bf16[1024,2048]{1,0:T(8,128)(2,1)} %bitcast.9, s32[1024]{0:T(1024)S(1)} %pad_clamp_fusion), kind=kCustom, calls=%fused_computation | custom fusion | bytes 4196352 | tf_op jit(solution)/shard_map/gather | solution.py:33
  237.4 4.0 %reshape.81 = f32[256,2,2048]{2,1,0:T(2,128)} reshape(bf16[512,2048]{1,0:T(8,128)(2,1)S(1)} %gather_fusion) | data formatting | bytes 6291456 | tf_op jit(solution)/shard_map/convert_element_type | solution.py:33
  241.4 9.9 %multiply_reduce_fusion = bf16[256,2048]{1,0:T(8,128)(2,1)} fusion(f32[256,2,2048]{2,1,0:T(2,128)} %reshape.81, f32[256,2]{1,0:T(8,128)S(1)} %copy.13), kind=kLoop, calls=%fused_computation.8 | loop fusion | flops 1572864 | bytes 5244928 | tf_op jit(solution)/shard_map/reduce_sum | solution.py:34
  (14 shorter events, 0.1 us)
Async XLA Ops:
  17.4 99.0 %copy-start.1 = (bf16[1,2048,1024]{2,1,0:T(8,128)(2,1)S(1)}, bf16[1,2048,1024]{2,1,0:T(8,128)(2,1)}, u32[]{:S(2)}) copy-start(bf16[1,2048,1024]{2,1,0:T(8,128)(2,1)} %param.12) | copy-start | bytes 12582916
  116.4 4.5 %copy-start.2 = (bf16[1,2048,1024]{2,1,0:T(8,128)(2,1)S(1)}, bf16[1,2048,1024]{2,1,0:T(8,128)(2,1)}, u32[]{:S(2)}) copy-start(bf16[1,2048,1024]{2,1,0:T(8,128)(2,1)} %param.11) | copy-start | bytes 12582916
  121.0 5.4 %copy-start.3 = (bf16[1,1024,2048]{2,1,0:T(8,128)(2,1)S(1)}, bf16[1,1024,2048]{2,1,0:T(8,128)(2,1)}, u32[]{:S(2)}) copy-start(bf16[1,1024,2048]{2,1,0:T(8,128)(2,1)} %param.13) | copy-start | bytes 12582916
  132.4 5.4 %copy-start = (f32[256,2]{0,1:T(2,128)S(1)}, f32[256,2]{0,1:T(2,128)}, u32[]{:S(2)}) copy-start(f32[256,2]{0,1:T(2,128)} %param.10) | copy-start | bytes 6148
  132.4 97.8 %all-to-all-start.1 = ((bf16[16,64,2048]{2,1,0:T(8,128)(2,1)}), bf16[16,64,2048]{2,1,0:T(8,128)(2,1)}, u32[]{:S(2)}, u32[]{:S(2)}) async-start(bf16[16,64,2048]{2,1,0:T(8,128)(2,1)} %bitcast.42), calls=%async_computation.1 | async-start | bytes 8388608 | tf_op jit(solution)/shard_map/all_to_all | solution.py:31
where the time goes:
time: 252 us; the launch traced here: 251 us
  blocking collectives  99 us (39%)
  waiting for transfers between devices  92.3 us (37%)
  local copies, waits for them, and re-layouts  23.6 us (9%)
  matrix products  16 us (6%)
  other arithmetic  14.9 us (6%)
  starting transfers between devices  5.35 us (2%)
    all_to_all x1, blocking collectives, per_device(): lax.all_to_all(outgoing, 'ep', split_axis=0, concat_axis=0, tiled=True)  99 us
    all_to_all x1, waiting for transfers between devices, per_device(): lax.all_to_all(finished, 'ep', split_axis=0, concat_axis=0, tiled=True)  92.3 us
    reduce_sum x1, other arithmetic, per_device(): mixed = jnp.sum(back * gate_weights[:, :, None], axis=1)  9.86 us
    scatter x1, local copies, waits for them, and re-layouts, per_device(): jnp.zeros((experts * capacity, feature_width), jnp.bfloat16).at[dest]  7.21 us
    gather x1, local copies, waits for them, and re-layouts, per_device(): returned[dest].astype(jnp.float32)  7.13 us
    dot_general x1, matrix products, per_device(): jnp.dot(hidden, w_down[0], preferred_element_type=jnp.float32)  6.09 us
    dot_general x1, matrix products, per_device(): gate = jnp.dot(rows, w_gate[0], preferred_element_type=jnp.float32)  5.35 us
    all_to_all x1, starting transfers between devices, per_device(): lax.all_to_all(finished, 'ep', split_axis=0, concat_axis=0, tiled=True)  5.35 us
  transfers between devices with their start and end apart: 1, of which 1 were waited for; matrix products, arithmetic and copies ran while one was open for 0% of the time, Pallas kernels for 0%

commit v1 on v0

v1 whole, which is shorter than its diff:
```python
import functools
import jax
import jax.numpy as jnp
from jax import lax
from jax.experimental import pallas as pl
from jax.experimental.pallas import tpu as pltpu
from jax.sharding import PartitionSpec as P

SUB = 4


def kernel(n, cap, tok_ref, gain_ref, ids_ref, gw_ref, wg_ref, wu_ref, wd_ref, out_ref,
           wg, wu, wd, normed, outgoing, arrived, results, returned, hidden, acc,
           send1, recv1, send2, recv2, wsem):
    zs = n // SUB
    me = lax.axis_index("ep")
    hi, lo = me // SUB, me % SUB
    tok, width = tok_ref.shape
    ff = wg.shape[1]
    rows = SUB * cap

    barrier = pltpu.get_barrier_semaphore()

    def greet(r, carry):
        pl.semaphore_signal(barrier, inc=1, device_id={"ep": (me + r) % n},
                            device_id_type=pl.DeviceIdType.MESH)
        return carry

    lax.fori_loop(1, n, greet, 0)
    w_copies = [
        pltpu.make_async_copy(wg_ref.at[0], wg, wsem.at[0]),
        pltpu.make_async_copy(wu_ref.at[0], wu, wsem.at[1]),
        pltpu.make_async_copy(wd_ref.at[0], wd, wsem.at[2]),
    ]
    for c in w_copies:
        c.start()

    ids = ids_ref[...]
    id0, id1 = ids[:, 0:1], ids[:, 1:2]
    lane = lax.broadcasted_iota(jnp.int32, (tok, 128), 1)
    chosen = jnp.where((id0 == lane) | (id1 == lane), 1.0, 0.0)
    t_row = lax.broadcasted_iota(jnp.int32, (tok, tok), 0)
    t_col = lax.broadcasted_iota(jnp.int32, (tok, tok), 1)
    earlier = jnp.where(t_col < t_row, 1.0, 0.0).astype(jnp.bfloat16)
    before = jnp.dot(earlier, chosen.astype(jnp.bfloat16), preferred_element_type=jnp.float32)
    slot0 = jnp.sum(jnp.where(id0 == lane, before, 0.0), axis=1, keepdims=True)
    slot1 = jnp.sum(jnp.where(id1 == lane, before, 0.0), axis=1, keepdims=True)
    dest0 = id0.astype(jnp.float32) * cap + slot0
    dest1 = id1.astype(jnp.float32) * cap + slot1
    both = jnp.where(lane == 0, dest0, jnp.where(lane == 1, dest1, 0.0))
    turned = jnp.transpose(both)
    row0 = turned[0:1, :].astype(jnp.int32)
    row1 = turned[1:2, :].astype(jnp.int32)
    col0 = dest0.astype(jnp.int32)
    col1 = dest1.astype(jnp.int32)

    step = 32

    def norm(i, carry):
        at = pl.ds(pl.multiple_of(i * step, step), step)
        v = tok_ref[at, :].astype(jnp.float32)
        scale = lax.rsqrt(jnp.mean(v * v, -1, keepdims=True) + 1e-06)
        normed[at, :] = (v * scale * gain_ref[...]).astype(jnp.bfloat16)
        return carry

    lax.fori_loop(0, tok // step, norm, 0)

    def shift(j):
        return ((j % 2) * ((j + 1) // 2) + (1 - j % 2) * (zs - j // 2)) % zs

    def target(dz, dl):
        return ((hi + dz) % zs) * SUB + (lo + dl) % SUB

    def source(dz, dl):
        return ((hi - dz + zs) % zs) * SUB + (lo - dl + SUB) % SUB

    def slot_rows(j, dl):
        return pl.ds(pl.multiple_of(j * rows + dl * cap, cap), cap)

    def out_copy(j, dl):
        at = slot_rows(j, dl)
        return pltpu.make_async_remote_copy(
            src_ref=outgoing.at[at, :], dst_ref=arrived.at[at, :],
            send_sem=send1.at[j * SUB + dl], recv_sem=recv1.at[j * SUB + dl],
            device_id={"ep": target(shift(j), dl)}, device_id_type=pl.DeviceIdType.MESH)

    def back_copy(j, dl):
        at = slot_rows(j, dl)
        return pltpu.make_async_remote_copy(
            src_ref=results.at[at, :], dst_ref=returned.at[at, :],
            send_sem=send2.at[j * SUB + dl], recv_sem=recv2.at[j * SUB + dl],
            device_id={"ep": source(shift(j), dl)}, device_id_type=pl.DeviceIdType.MESH)

    def chunk_rows(j):
        return pl.ds(pl.multiple_of(j * rows, rows), rows)

    def pack(j):
        r = lax.broadcasted_iota(jnp.int32, (rows, tok), 0)
        dl, s = r // cap, r % cap
        expert = ((hi + shift(j)) % zs) * SUB + (lo + dl) % SUB
        index = expert * cap + s
        pick = jnp.where((index == row0) | (index == row1), 1.0, 0.0).astype(jnp.bfloat16)
        outgoing[chunk_rows(j), :] = jnp.dot(
            pick, normed[...], preferred_element_type=jnp.float32).astype(jnp.bfloat16)

    def send_out(j):
        for dl in range(SUB):
            out_copy(j, dl).start()

    pack(0)
    pl.semaphore_wait(barrier, n - 1)
    for dl in range(1, SUB):
        out_copy(0, dl).start()
    arrived[0:cap, :] = outgoing[0:cap, :]

    def dispatch(j, carry):
        pack(j)
        send_out(j)
        return carry

    lax.fori_loop(1, zs, dispatch, 0)

    for c in w_copies:
        c.wait()

    ftile = min(ff, 256)
    dtile = min(width, 256)

    def experts(j):
        at = chunk_rows(j)

        def up(f, carry):
            cols = pl.ds(pl.multiple_of(f * ftile, ftile), ftile)
            x = arrived[at, :]
            g = jnp.dot(x, wg[:, cols], preferred_element_type=jnp.float32)
            u = jnp.dot(x, wu[:, cols], preferred_element_type=jnp.float32)
            hidden[:, cols] = (g / (1.0 + jnp.exp(-g)) * u).astype(jnp.bfloat16)
            return carry

        lax.fori_loop(0, ff // ftile, up, 0)

        def down(d, carry):
            cols = pl.ds(pl.multiple_of(d * dtile, dtile), dtile)
            results[at, cols] = jnp.dot(
                hidden[...], wd[:, cols], preferred_element_type=jnp.float32).astype(jnp.bfloat16)
            return carry

        lax.fori_loop(0, width // dtile, down, 0)

    for dl in range(1, SUB):
        out_copy(0, dl).wait_recv()
    experts(0)
    for dl in range(1, SUB):
        back_copy(0, dl).start()
    returned[0:cap, :] = results[0:cap, :]

    def work(j, carry):
        for dl in range(SUB):
            out_copy(j, dl).wait_recv()
        experts(j)
        for dl in range(SUB):
            back_copy(j, dl).start()
        return carry

    lax.fori_loop(1, zs, work, 0)

    gw = gw_ref[...]
    g0, g1 = gw[:, 0:1], gw[:, 1:2]

    def gather(j):
        c = lax.broadcasted_iota(jnp.int32, (tok, rows), 1)
        dl, s = c // cap, c % cap
        expert = ((hi + shift(j)) % zs) * SUB + (lo + dl) % SUB
        index = expert * cap + s
        weight = jnp.where(index == col0, g0, 0.0) + jnp.where(index == col1, g1, 0.0)
        high = weight.astype(jnp.bfloat16)
        low = (weight - high.astype(jnp.float32)).astype(jnp.bfloat16)
        block = returned[chunk_rows(j), :]
        return (jnp.dot(high, block, preferred_element_type=jnp.float32)
                + jnp.dot(low, block, preferred_element_type=jnp.float32))

    for dl in range(1, SUB):
        back_copy(0, dl).wait_recv()
    acc[...] = gather(0)

    def combine(j, carry):
        for dl in range(SUB):
            back_copy(j, dl).wait_recv()
        acc[...] += gather(j)
        return carry

    lax.fori_loop(1, zs - 1, combine, 0)
    for dl in range(SUB):
        back_copy(zs - 1, dl).wait_recv()
    out_ref[...] = (acc[...] + gather(zs - 1)).astype(out_ref.dtype)

    for dl in range(1, SUB):
        out_copy(0, dl).wait_send()
        back_copy(0, dl).wait_send()

    def finish(j, carry):
        for dl in range(SUB):
            out_copy(j, dl).wait_send()
            back_copy(j, dl).wait_send()
        return carry

    lax.fori_loop(1, zs, finish, 0)


def per_device(tokens, norm_gain, expert_ids, gate_weights, w_gate, w_up, w_down):
    n = lax.axis_size("ep")
    tok, width = tokens.shape
    top = expert_ids.shape[1]
    ff = w_gate.shape[2]
    cap = 2 * tok * top // n
    total = n * cap
    bf16 = jnp.bfloat16
    vmem = pl.BlockSpec(memory_space=pltpu.VMEM)
    hbm = pl.BlockSpec(memory_space=pl.ANY)
    return pl.pallas_call(
        functools.partial(kernel, n, cap),
        out_shape=jax.ShapeDtypeStruct((tok, width), bf16),
        in_specs=[vmem] * 4 + [hbm] * 3,
        out_specs=vmem,
        scratch_shapes=[
            pltpu.VMEM((width, ff), bf16),
            pltpu.VMEM((width, ff), bf16),
            pltpu.VMEM((ff, width), bf16),
            pltpu.VMEM((tok, width), bf16),
            pltpu.VMEM((total, width), bf16),
            pltpu.VMEM((total, width), bf16),
            pltpu.VMEM((total, width), bf16),
            pltpu.VMEM((total, width), bf16),
            pltpu.VMEM((SUB * cap, ff), bf16),
            pltpu.VMEM((tok, width), jnp.float32),
            pltpu.SemaphoreType.DMA((n,)),
            pltpu.SemaphoreType.DMA((n,)),
            pltpu.SemaphoreType.DMA((n,)),
            pltpu.SemaphoreType.DMA((n,)),
            pltpu.SemaphoreType.DMA((3,)),
        ],
        compiler_params=pltpu.CompilerParams(
            collective_id=0, has_side_effects=True, vmem_limit_bytes=56 * 1024 * 1024),
    )(tokens, norm_gain.reshape(1, width), expert_ids, gate_weights, w_gate, w_up, w_down)


def solution(mesh):
    return jax.shard_map(
        per_device,
        mesh=mesh,
        in_specs=(
            P(("grp", "ep"), None),
            P(),
            P(("grp", "ep"), None),
            P(("grp", "ep"), None),
            P("ep", None, None),
            P("ep", None, None),
            P("ep", None, None),
        ),
        out_specs=P(("grp", "ep"), None),
        check_vma=False,
    )
```

time: 252 us -> 197 us (0.78)
  the two profiles are of different devices: /device:TPU:15 before, /device:TPU:1 now
where the time goes in v1:
time: 197 us; the launch traced here: 196 us
  Pallas kernels  191 us (97%)
  local copies, waits for them, and re-layouts  5.24 us (3%)
    pallas_call x1, Pallas kernels, per_device(): pl.pallas_call(functools.partial(kernel, n, cap), out_shape=jax.ShapeDtyp...  191 us
    unnamed x3, local copies, waits for them, and re-layouts  5.24 us

profile of v1, /device:TPU:1, one launch (start us, length us, event | category | flops | bytes accessed | tf_op | source)
XLA Modules:
  0.0 196.4 jit_solution(10287070907120858805)
XLA Ops:
  0.0 1.5 copy.8.ids_ref
  1.5 1.5 copy.9.gw_ref
  2.9 191.2 %shard_map.73 = bf16[256,2048]{1,0:T(8,128)(2,1)} custom-call(bf16[256,2048]{1,0:T(8,128)(2,1)} %tok_ref.1, f32[1,2048]{1,0:T(1,128)} %bitcast.1, s32[256,2]{1,0:T(8,128)} %copy.8.ids_ref, f32[256,2]{1,0:T(8,128)} %copy.9.gw_ref, bf16[1,2048,1024]{2,1,0:T(8,128)(2,1)} %wg_ref.1, bf16[1,2048,1024]{2,1,0:T(8,128)(2,1)} %wu_ref.1, bf16[1,1024,2048]{2,1,0:T(8,128)(2,1)} %wd_ref.1), custom_call_target="tpu_custom_call" | custom-call | tf_op jit(solution)/shard_map/pallas_call | solution.py:220
  194.1 2.3 %copy.11 = bf16[256,2048]{1,0:T(8,128)(2,1)} copy(bf16[256,2048]{1,0:T(8,128)(2,1)} %shard_map.73) | data formatting | bytes 2097152

commit v2 on v1

--- a/solution.py
+++ b/solution.py
@@ -10,8 +10,9 @@
 
 
 def kernel(n, cap, tok_ref, gain_ref, ids_ref, gw_ref, wg_ref, wu_ref, wd_ref, out_ref,
-           wg, wu, wd, normed, outgoing, arrived, results, returned, hidden, acc,
-           send1, recv1, send2, recv2, wsem):
+           wg, wu, wd, lines, places, outgoing, arrived, results, returned, hidden, acc,
+           send1, recv1, send2, recv2, wsem,
+           lsend, lrecv, psend, precv):
     zs = n // SUB
     me = lax.axis_index("ep")
     hi, lo = me // SUB, me % SUB
@@ -49,10 +50,6 @@
     dest1 = id1.astype(jnp.float32) * cap + slot1
     both = jnp.where(lane == 0, dest0, jnp.where(lane == 1, dest1, 0.0))
     turned = jnp.transpose(both)
-    row0 = turned[0:1, :].astype(jnp.int32)
-    row1 = turned[1:2, :].astype(jnp.int32)
-    col0 = dest0.astype(jnp.int32)
-    col1 = dest1.astype(jnp.int32)
 
     step = 32
 
@@ -60,74 +57,75 @@
         at = pl.ds(pl.multiple_of(i * step, step), step)
         v = tok_ref[at, :].astype(jnp.float32)
         scale = lax.rsqrt(jnp.mean(v * v, -1, keepdims=True) + 1e-06)
-        normed[at, :] = (v * scale * gain_ref[...]).astype(jnp.bfloat16)
+        lines[hi, at, :] = (v * scale * gain_ref[...]).astype(jnp.bfloat16)
         return carry
 
     lax.fori_loop(0, tok // step, norm, 0)
 
-    def shift(j):
-        return ((j % 2) * ((j + 1) // 2) + (1 - j % 2) * (zs - j // 2)) % zs
-
-    def target(dz, dl):
-        return ((hi + dz) % zs) * SUB + (lo + dl) % SUB
-
-    def source(dz, dl):
-        return ((hi - dz + zs) % zs) * SUB + (lo - dl + SUB) % SUB
+    def wait_all(copies):
+        for c in copies:
+            c.wait_recv()
+
+    def line_copies(block, way):
+        to = (hi + 2 * way - 1 + zs) % zs * SUB + lo
+        return [
+            pltpu.make_async_remote_copy(
+                src_ref=buf.at[block], dst_ref=buf.at[block],
+                send_sem=sends.at[way * zs + block], recv_sem=recvs.at[block],
+                device_id={"ep": to}, device_id_type=pl.DeviceIdType.MESH)
+            for buf, sends, recvs in ((places, psend, precv), (lines, lsend, lrecv))
+        ]
+
+    def pass_on(block, way):
+        for c in line_copies(block, way):
+            c.start()
 
     def slot_rows(j, dl):
         return pl.ds(pl.multiple_of(j * rows + dl * cap, cap), cap)
+
+    def chunk_rows(j):
+        return pl.ds(pl.multiple_of(j * rows, rows), rows)
 
     def out_copy(j, dl):
         at = slot_rows(j, dl)
         return pltpu.make_async_remote_copy(
             src_ref=outgoing.at[at, :], dst_ref=arrived.at[at, :],
             send_sem=send1.at[j * SUB + dl], recv_sem=recv1.at[j * SUB + dl],
-            device_id={"ep": target(shift(j), dl)}, device_id_type=pl.DeviceIdType.MESH)
+            device_id={"ep": hi * SUB + (lo + dl) % SUB}, device_id_type=pl.DeviceIdType.MESH)
 
     def back_copy(j, dl):
+        return pltpu.make_async_remote_copy(
+            src_ref=results.at[slot_rows(j, dl), :], dst_ref=returned.at[slot_rows(hi, dl), :],
+            send_sem=send2.at[j * SUB + dl], recv_sem=recv2.at[hi * SUB + dl],
+            device_id={"ep": j * SUB + (lo - dl + SUB) % SUB}, device_id_type=pl.DeviceIdType.MESH)
+
+    def back_arrival(j, dl):
         at = slot_rows(j, dl)
         return pltpu.make_async_remote_copy(
             src_ref=results.at[at, :], dst_ref=returned.at[at, :],
             send_sem=send2.at[j * SUB + dl], recv_sem=recv2.at[j * SUB + dl],
-            device_id={"ep": source(shift(j), dl)}, device_id_type=pl.DeviceIdType.MESH)
-
-    def chunk_rows(j):
-        return pl.ds(pl.multiple_of(j * rows, rows), rows)
+            device_id={"ep": j * SUB + (lo + dl) % SUB}, device_id_type=pl.DeviceIdType.MESH)
 
     def pack(j):
         r = lax.broadcasted_iota(jnp.int32, (rows, tok), 0)
         dl, s = r // cap, r % cap
-        expert = ((hi + shift(j)) % zs) * SUB + (lo + dl) % SUB
-        index = expert * cap + s
-        pick = jnp.where((index == row0) | (index == row1), 1.0, 0.0).astype(jnp.bfloat16)
+        index = ((hi * SUB + (lo + dl) % SUB) * cap + s).astype(jnp.float32)
+        where = places[j]
+        pick = jnp.where((index == where[0:1, :]) | (index == where[1:2, :]), 1.0, 0.0)
         outgoing[chunk_rows(j), :] = jnp.dot(
-            pick, normed[...], preferred_element_type=jnp.float32).astype(jnp.bfloat16)
-
-    def send_out(j):
-        for dl in range(SUB):
+            pick.astype(jnp.bfloat16), lines[j], preferred_element_type=jnp.float32
+        ).astype(jnp.bfloat16)
+        for dl in range(1, SUB):
             out_copy(j, dl).start()
-
-    pack(0)
-    pl.semaphore_wait(barrier, n - 1)
-    for dl in range(1, SUB):
-        out_copy(0, dl).start()
-    arrived[0:cap, :] = outgoing[0:cap, :]
-
-    def dispatch(j, carry):
-        pack(j)
-        send_out(j)
-        return carry
-
-    lax.fori_loop(1, zs, dispatch, 0)
-
-    for c in w_copies:
-        c.wait()
+        arrived[slot_rows(j, 0), :] = outgoing[slot_rows(j, 0), :]
 
     ftile = min(ff, 256)
     dtile = min(width, 256)
 
     def experts(j):
         at = chunk_rows(j)
+        for dl in range(1, SUB):
+            out_copy(j, dl).wait_recv()
 
         def up(f, carry):
             cols = pl.ds(pl.multiple_of(f * ftile, ftile), ftile)
@@ -146,23 +144,63 @@
             return carry
 
         lax.fori_loop(0, width // dtile, down, 0)
-
-    for dl in range(1, SUB):
-        out_copy(0, dl).wait_recv()
-    experts(0)
-    for dl in range(1, SUB):
-        back_copy(0, dl).start()
-    returned[0:cap, :] = results[0:cap, :]
-
-    def work(j, carry):
-        for dl in range(SUB):
-            out_copy(j, dl).wait_recv()
-        experts(j)
-        for dl in range(SUB):
+        for dl in range(1, SUB):
             back_copy(j, dl).start()
-        return carry
-
-    lax.fori_loop(1, zs, work, 0)
+
+        @pl.when(j == hi)
+        def _():
+            returned[slot_rows(hi, 0), :] = results[slot_rows(hi, 0), :]
+
+        @pl.when(j != hi)
+        def _():
+            back_copy(j, 0).start()
+
+    def both_sides(s, act):
+        @pl.when(hi - s >= 0)
+        def _():
+            act((hi - s + zs) % zs, 1)
+
+        @pl.when(hi + s < zs)
+        def _():
+            act((hi + s) % zs, 0)
+
+    def forward(block, way):
+        @pl.when(hi < zs - 1 if way else hi > 0)
+        def _():
+            pass_on(block, way)
+
+    def line_arrival(block, way):
+        wait_all(line_copies(block, way))
+
+    where = lax.broadcasted_iota(jnp.int32, (8, tok), 0)
+    places[hi] = jnp.where(where == 0, turned[0:1, :], turned[1:2, :])
+    pl.semaphore_wait(barrier, n - 1)
+    forward(hi, 1)
+    forward(hi, 0)
+    pack(hi)
+    for c in w_copies:
+        c.wait()
+
+    def step_in(s, carry):
+        def take(block, way):
+            line_arrival(block, way)
+            forward(block, way)
+
+        both_sides(s, take)
+        both_sides(s, lambda block, way: pack(block))
+
+        @pl.when(s == 1)
+        def _():
+            experts(hi)
+
+        @pl.when(s > 1)
+        def _():
+            both_sides(s - 1, lambda block, way: experts(block))
+
+        return carry
+
+    lax.fori_loop(1, zs, step_in, 0)
+    both_sides(zs - 1, lambda block, way: experts(block))
 
     gw = gw_ref[...]
     g0, g1 = gw[:, 0:1], gw[:, 1:2]
@@ -170,41 +208,46 @@
     def gather(j):
         c = lax.broadcasted_iota(jnp.int32, (tok, rows), 1)
         dl, s = c // cap, c % cap
-        expert = ((hi + shift(j)) % zs) * SUB + (lo + dl) % SUB
-        index = expert * cap + s
-        weight = jnp.where(index == col0, g0, 0.0) + jnp.where(index == col1, g1, 0.0)
+        index = ((j * SUB + (lo + dl) % SUB) * cap + s).astype(jnp.float32)
+        weight = jnp.where(index == dest0, g0, 0.0) + jnp.where(index == dest1, g1, 0.0)
         high = weight.astype(jnp.bfloat16)
         low = (weight - high.astype(jnp.float32)).astype(jnp.bfloat16)
         block = returned[chunk_rows(j), :]
         return (jnp.dot(high, block, preferred_element_type=jnp.float32)
                 + jnp.dot(low, block, preferred_element_type=jnp.float32))
 
-    for dl in range(1, SUB):
-        back_copy(0, dl).wait_recv()
-    acc[...] = gather(0)
-
-    def combine(j, carry):
-        for dl in range(SUB):
-            back_copy(j, dl).wait_recv()
-        acc[...] += gather(j)
-        return carry
-
-    lax.fori_loop(1, zs - 1, combine, 0)
-    for dl in range(SUB):
-        back_copy(zs - 1, dl).wait_recv()
-    out_ref[...] = (acc[...] + gather(zs - 1)).astype(out_ref.dtype)
-
-    for dl in range(1, SUB):
-        out_copy(0, dl).wait_send()
-        back_copy(0, dl).wait_send()
+    wait_all([back_arrival(hi, dl) for dl in range(1, SUB)])
+    acc[...] = gather(hi)
+
+    def combine(s, carry):
+        def add(block, way):
+            wait_all([back_arrival(block, dl) for dl in range(SUB)])
+            acc[...] += gather(block)
+
+        both_sides(s, add)
+        return carry
+
+    lax.fori_loop(1, zs, combine, 0)
+    out_ref[...] = acc[...].astype(out_ref.dtype)
 
     def finish(j, carry):
-        for dl in range(SUB):
+        for dl in range(1, SUB):
             out_copy(j, dl).wait_send()
             back_copy(j, dl).wait_send()
-        return carry
-
-    lax.fori_loop(1, zs, finish, 0)
+
+        @pl.when(j != hi)
+        def _():
+            back_copy(j, 0).wait_send()
+
+        for way in (0, 1):
+            @pl.when((hi < zs - 1) & (j <= hi) if way else (hi > 0) & (j >= hi))
+            def _():
+                for c in line_copies(j, way):
+                    c.wait_send()
+
+        return carry
+
+    lax.fori_loop(0, zs, finish, 0)
 
 
 def per_device(tokens, norm_gain, expert_ids, gate_weights, w_gate, w_up, w_down):
@@ -226,7 +269,8 @@
             pltpu.VMEM((width, ff), bf16),
             pltpu.VMEM((width, ff), bf16),
             pltpu.VMEM((ff, width), bf16),
-            pltpu.VMEM((tok, width), bf16),
+            pltpu.VMEM((n // SUB, tok, width), bf16),
+            pltpu.VMEM((n // SUB, 8, tok), jnp.float32),
             pltpu.VMEM((total, width), bf16),
             pltpu.VMEM((total, width), bf16),
             pltpu.VMEM((total, width), bf16),
@@ -238,6 +282,10 @@
             pltpu.SemaphoreType.DMA((n,)),
             pltpu.SemaphoreType.DMA((n,)),
             pltpu.SemaphoreType.DMA((3,)),
+            pltpu.SemaphoreType.DMA((2 * n // SUB,)),
+            pltpu.SemaphoreType.DMA((n // SUB,)),
+            pltpu.SemaphoreType.DMA((2 * n // SUB,)),
+            pltpu.SemaphoreType.DMA((n // SUB,)),
         ],
         compiler_params=pltpu.CompilerParams(
             collective_id=0, has_side_effects=True, vmem_limit_bytes=56 * 1024 * 1024),

time: 197 us -> 170 us (0.86)
  Pallas kernels: 191 us -> 163 us
    pallas_call x1, Pallas kernels: 191 us -> 163 us  [per_device(): pl.pallas_call(functools.partial(kernel, n, cap), out_shape=jax.ShapeDtyp...]
where the time goes in v2:
time: 170 us; the launch traced here: 168 us
  Pallas kernels  163 us (96%)
  local copies, waits for them, and re-layouts  5.24 us (3%)
    pallas_call x1, Pallas kernels, per_device(): pl.pallas_call(functools.partial(kernel, n, cap), out_shape=jax.ShapeDtyp...  163 us
    unnamed x3, local copies, waits for them, and re-layouts  5.24 us

profile of v2, /device:TPU:1, one launch (start us, length us, event | category | flops | bytes accessed | tf_op | source)
XLA Modules:
  0.0 168.0 jit_solution(2773567923377840573)
XLA Ops:
  0.0 1.5 copy.8.ids_ref
  1.5 1.5 copy.9.gw_ref
  2.9 162.8 %shard_map.73 = bf16[256,2048]{1,0:T(8,128)(2,1)} custom-call(bf16[256,2048]{1,0:T(8,128)(2,1)} %tok_ref.1, f32[1,2048]{1,0:T(1,128)} %bitcast.1, s32[256,2]{1,0:T(8,128)} %copy.8.ids_ref, f32[256,2]{1,0:T(8,128)} %copy.9.gw_ref, bf16[1,2048,1024]{2,1,0:T(8,128)(2,1)} %wg_ref.1, bf16[1,2048,1024]{2,1,0:T(8,128)(2,1)} %wu_ref.1, bf16[1,1024,2048]{2,1,0:T(8,128)(2,1)} %wd_ref.1), custom_call_target="tpu_custom_call" | custom-call | tf_op jit(solution)/shard_map/pallas_call | solution.py:263
  165.7 2.3 %copy.11 = bf16[256,2048]{1,0:T(8,128)(2,1)} copy(bf16[256,2048]{1,0:T(8,128)(2,1)} %shard_map.73) | data formatting | bytes 2097152

commit v3 on v2

--- a/solution.py
+++ b/solution.py
@@ -181,26 +181,35 @@
     for c in w_copies:
         c.wait()
 
+    experts(hi)
+
+    side = 1 - 2 * (hi // ((zs + 1) // 2))
+
+    def along(s, act):
+        block = hi + side * s
+
+        @pl.when((block >= 0) & (block < zs))
+        def _():
+            act((block + zs) % zs)
+
     def step_in(s, carry):
         def take(block, way):
             line_arrival(block, way)
             forward(block, way)
 
         both_sides(s, take)
-        both_sides(s, lambda block, way: pack(block))
-
-        @pl.when(s == 1)
-        def _():
-            experts(hi)
+        along(s, pack)
+        along(-s, pack)
 
         @pl.when(s > 1)
         def _():
-            both_sides(s - 1, lambda block, way: experts(block))
-
+            along(1 - s, experts)
+
+        along(s, experts)
         return carry
 
     lax.fori_loop(1, zs, step_in, 0)
-    both_sides(zs - 1, lambda block, way: experts(block))
+    along(1 - zs, experts)
 
     gw = gw_ref[...]
     g0, g1 = gw[:, 0:1], gw[:, 1:2]

time: 170 us -> 160 us (0.941)
  Pallas kernels: 163 us -> 153 us
    pallas_call x1, Pallas kernels: 163 us -> 153 us  [per_device(): pl.pallas_call(functools.partial(kernel, n, cap), out_shape=jax.ShapeDtyp...]
where the time goes in v3:
time: 160 us; the launch traced here: 159 us
  Pallas kernels  153 us (96%)
  local copies, waits for them, and re-layouts  5.24 us (3%)
    pallas_call x1, Pallas kernels, per_device(): pl.pallas_call(functools.partial(kernel, n, cap), out_shape=jax.ShapeDtyp...  153 us
    unnamed x3, local copies, waits for them, and re-layouts  5.24 us

profile of v3, /device:TPU:1, one launch (start us, length us, event | category | flops | bytes accessed | tf_op | source)
XLA Modules:
  0.0 158.5 jit_solution(3278187675219010009)
XLA Ops:
  0.0 1.5 copy.8.ids_ref
  1.5 1.5 copy.9.gw_ref
  2.9 153.3 %shard_map.73 = bf16[256,2048]{1,0:T(8,128)(2,1)} custom-call(bf16[256,2048]{1,0:T(8,128)(2,1)} %tok_ref.1, f32[1,2048]{1,0:T(1,128)} %bitcast.1, s32[256,2]{1,0:T(8,128)} %copy.8.ids_ref, f32[256,2]{1,0:T(8,128)} %copy.9.gw_ref, bf16[1,2048,1024]{2,1,0:T(8,128)(2,1)} %wg_ref.1, bf16[1,2048,1024]{2,1,0:T(8,128)(2,1)} %wu_ref.1, bf16[1,1024,2048]{2,1,0:T(8,128)(2,1)} %wd_ref.1), custom_call_target="tpu_custom_call" | custom-call | tf_op jit(solution)/shard_map/pallas_call | solution.py:272
  156.2 2.3 %copy.11 = bf16[256,2048]{1,0:T(8,128)(2,1)} copy(bf16[256,2048]{1,0:T(8,128)(2,1)} %shard_map.73) | data formatting | bytes 2097152

commit v4 on v3

--- a/solution.py
+++ b/solution.py
@@ -7,12 +7,14 @@
 from jax.sharding import PartitionSpec as P
 
 SUB = 4
+HALVES = 2
 
 
 def kernel(n, cap, tok_ref, gain_ref, ids_ref, gw_ref, wg_ref, wu_ref, wd_ref, out_ref,
            wg, wu, wd, lines, places, outgoing, arrived, results, returned, hidden, acc,
            send1, recv1, send2, recv2, wsem,
-           lsend, lrecv, psend, precv):
+           lsend, lrecv, psend, precv,
+           relay, dense, landed, rsend, rrecv, dsend, drecv):
     zs = n // SUB
     me = lax.axis_index("ep")
     hi, lo = me // SUB, me % SUB
@@ -48,7 +50,10 @@
     slot1 = jnp.sum(jnp.where(id1 == lane, before, 0.0), axis=1, keepdims=True)
     dest0 = id0.astype(jnp.float32) * cap + slot0
     dest1 = id1.astype(jnp.float32) * cap + slot1
-    both = jnp.where(lane == 0, dest0, jnp.where(lane == 1, dest1, 0.0))
+    gw = gw_ref[...]
+    g0, g1 = gw[:, 0:1], gw[:, 1:2]
+    both = jnp.where(lane == 0, dest0, jnp.where(
+        lane == 1, dest1, jnp.where(lane == 2, g0, jnp.where(lane == 3, g1, 0.0))))
     turned = jnp.transpose(both)
 
     step = 32
@@ -119,6 +124,49 @@
             out_copy(j, dl).start()
         arrived[slot_rows(j, 0), :] = outgoing[slot_rows(j, 0), :]
 
+    upper = hi // (zs - 2)
+    meet = upper * (zs - 2) + (1 - upper)
+    part = upper * (hi - (zs - 2)) + (1 - upper) * (1 - hi)
+    half = width // HALVES
+
+    def direct(plane, block):
+        return jnp.logical_not(((plane >= zs - 2) & (block < zs - 2)) | ((plane <= 1) & (block > 1)))
+
+    def relay_copy(j, dl, h):
+        at = j - 2 * (1 - upper)
+        cols = pl.ds(h * half, half)
+        return pltpu.make_async_remote_copy(
+            src_ref=results.at[slot_rows(j, dl), cols],
+            dst_ref=relay.at[part, slot_rows(at, dl), cols],
+            send_sem=rsend.at[(at * SUB + dl) * HALVES + h],
+            recv_sem=rrecv.at[((part * (zs - 2) + at) * SUB + dl) * HALVES + h],
+            device_id={"ep": meet * SUB + (lo - dl + SUB) % SUB},
+            device_id_type=pl.DeviceIdType.MESH)
+
+    def relay_arrival(p, at, dl, h):
+        cols = pl.ds(h * half, half)
+        sem = ((p * (zs - 2) + at) * SUB + dl) * HALVES + h
+        return pltpu.make_async_remote_copy(
+            src_ref=relay.at[p, slot_rows(at, dl), cols],
+            dst_ref=relay.at[p, slot_rows(at, dl), cols],
+            send_sem=rsend.at[(at * SUB + dl) * HALVES + h], recv_sem=rrecv.at[sem],
+            device_id={"ep": meet * SUB + (lo + 1) % SUB}, device_id_type=pl.DeviceIdType.MESH)
+
+    def dense_copy(at, h):
+        cols = pl.ds(h * half, half)
+        return pltpu.make_async_remote_copy(
+            src_ref=dense.at[at, :, cols], dst_ref=landed.at[upper, :, cols],
+            send_sem=dsend.at[at * HALVES + h], recv_sem=drecv.at[upper * HALVES + h],
+            device_id={"ep": (at + 2 * (1 - upper)) * SUB + lo},
+            device_id_type=pl.DeviceIdType.MESH)
+
+    def dense_arrival(end, h):
+        cols = pl.ds(h * half, half)
+        return pltpu.make_async_remote_copy(
+            src_ref=landed.at[end, :, cols], dst_ref=landed.at[end, :, cols],
+            send_sem=dsend.at[h], recv_sem=drecv.at[end * HALVES + h],
+            device_id={"ep": (me + 1) % n}, device_id_type=pl.DeviceIdType.MESH)
+
     ftile = min(ff, 256)
     dtile = min(width, 256)
 
@@ -144,16 +192,33 @@
             return carry
 
         lax.fori_loop(0, width // dtile, down, 0)
-        for dl in range(1, SUB):
-            back_copy(j, dl).start()
+
+        @pl.when(direct(hi, j))
+        def _():
+            for dl in range(1, SUB):
+                back_copy(j, dl).start()
 
         @pl.when(j == hi)
         def _():
             returned[slot_rows(hi, 0), :] = results[slot_rows(hi, 0), :]
 
-        @pl.when(j != hi)
+        @pl.when((j != hi) & direct(hi, j))
         def _():
             back_copy(j, 0).start()
+
+        @pl.when(jnp.logical_not(direct(hi, j)))
+        def _():
+            for h in range(HALVES):
+                for dl in range(1, SUB):
+                    relay_copy(j, dl, h).start()
+
+                @pl.when(hi != meet)
+                def _():
+                    relay_copy(j, 0, h).start()
+
+            @pl.when(hi == meet)
+            def _():
+                relay[0, slot_rows(j - 2 * (1 - upper), 0), :] = results[slot_rows(j, 0), :]
 
     def both_sides(s, act):
         @pl.when(hi - s >= 0)
@@ -173,7 +238,9 @@
         wait_all(line_copies(block, way))
 
     where = lax.broadcasted_iota(jnp.int32, (8, tok), 0)
-    places[hi] = jnp.where(where == 0, turned[0:1, :], turned[1:2, :])
+    places[hi] = jnp.where(
+        where == 0, turned[0:1, :], jnp.where(
+            where == 1, turned[1:2, :], jnp.where(where == 2, turned[2:3, :], turned[3:4, :])))
     pl.semaphore_wait(barrier, n - 1)
     forward(hi, 1)
     forward(hi, 0)
@@ -211,8 +278,34 @@
     lax.fori_loop(1, zs, step_in, 0)
     along(1 - zs, experts)
 
-    gw = gw_ref[...]
-    g0, g1 = gw[:, 0:1], gw[:, 1:2]
+    def share(p, at, cols):
+        block_places = places[at + 2 * (1 - upper)]
+        r = lax.broadcasted_iota(jnp.int32, (rows, tok), 0)
+        dl, s = r // cap, r % cap
+        plane = upper * (zs - 2 + p) + (1 - upper) * (1 - p)
+        index = ((plane * SUB + (lo + dl) % SUB) * cap + s).astype(jnp.float32)
+        weight = (jnp.where(index == block_places[0:1, :], block_places[2:3, :], 0.0)
+                  + jnp.where(index == block_places[1:2, :], block_places[3:4, :], 0.0))
+        high = weight.astype(jnp.bfloat16)
+        low = (weight - high.astype(jnp.float32)).astype(jnp.bfloat16)
+        block = relay[p, chunk_rows(at), cols]
+        dims = (((0,), (0,)), ((), ()))
+        return (lax.dot_general(high, block, dims, preferred_element_type=jnp.float32)
+                + lax.dot_general(low, block, dims, preferred_element_type=jnp.float32))
+
+    @pl.when(hi == meet)
+    def _():
+        def meeting(t, carry):
+            at = upper * (zs - 3 - t) + (1 - upper) * t
+            for h in range(HALVES):
+                cols = pl.ds(h * half, half)
+                wait_all([relay_arrival(0, at, dl, h) for dl in range(1, SUB)])
+                wait_all([relay_arrival(1, at, dl, h) for dl in range(SUB)])
+                dense[at, :, cols] = (share(0, at, cols) + share(1, at, cols)).astype(jnp.bfloat16)
+                dense_copy(at, h).start()
+            return carry
+
+        lax.fori_loop(0, zs - 2, meeting, 0)
 
     def gather(j):
         c = lax.broadcasted_iota(jnp.int32, (tok, rows), 1)
@@ -230,23 +323,50 @@
 
     def combine(s, carry):
         def add(block, way):
-            wait_all([back_arrival(block, dl) for dl in range(SUB)])
-            acc[...] += gather(block)
+            @pl.when(direct(block, hi))
+            def _():
+                wait_all([back_arrival(block, dl) for dl in range(SUB)])
+                acc[...] += gather(block)
 
         both_sides(s, add)
         return carry
 
     lax.fori_loop(1, zs, combine, 0)
+    for end in (0, 1):
+        @pl.when(hi < zs - 2 if end else hi > 1)
+        def _():
+            for h in range(HALVES):
+                cols = pl.ds(h * half, half)
+                dense_arrival(end, h).wait_recv()
+                acc[:, cols] += landed[end, :, cols].astype(jnp.float32)
     out_ref[...] = acc[...].astype(out_ref.dtype)
 
     def finish(j, carry):
         for dl in range(1, SUB):
             out_copy(j, dl).wait_send()
-            back_copy(j, dl).wait_send()
-
-        @pl.when(j != hi)
+
+        @pl.when(direct(hi, j))
+        def _():
+            for dl in range(1, SUB):
+                back_copy(j, dl).wait_send()
+
+        @pl.when((j != hi) & direct(hi, j))
         def _():
             back_copy(j, 0).wait_send()
+
+        @pl.when(jnp.logical_not(direct(hi, j)))
+        def _():
+            for h in range(HALVES):
+                for dl in range(1, SUB):
+                    relay_copy(j, dl, h).wait_send()
+
+                @pl.when(hi != meet)
+                def _():
+                    relay_copy(j, 0, h).wait_send()
+
+                @pl.when(hi == meet)
+                def _():
+                    dense_copy(j - 2 * (1 - upper), h).wait_send()
 
         for way in (0, 1):
             @pl.when((hi < zs - 1) & (j <= hi) if way else (hi > 0) & (j >= hi))
@@ -295,9 +415,16 @@
             pltpu.SemaphoreType.DMA((n // SUB,)),
             pltpu.SemaphoreType.DMA((2 * n // SUB,)),
             pltpu.SemaphoreType.DMA((n // SUB,)),
+            pltpu.VMEM((2, (n // SUB - 2) * SUB * cap, width), bf16),
+            pltpu.VMEM((n // SUB - 2, tok, width), bf16),
+            pltpu.VMEM((2, tok, width), bf16),
+            pltpu.SemaphoreType.DMA(((n - 2 * SUB) * HALVES,)),
+            pltpu.SemaphoreType.DMA((2 * (n - 2 * SUB) * HALVES,)),
+            pltpu.SemaphoreType.DMA(((n // SUB - 2) * HALVES,)),
+            pltpu.SemaphoreType.DMA((2 * HALVES,)),
         ],
         compiler_params=pltpu.CompilerParams(
-            collective_id=0, has_side_effects=True, vmem_limit_bytes=56 * 1024 * 1024),
+            collective_id=0, has_side_effects=True, vmem_limit_bytes=62 * 1024 * 1024),
     )(tokens, norm_gain.reshape(1, width), expert_ids, gate_weights, w_gate, w_up, w_down)
 
 

time: 160 us -> 159 us (level)
  no operation moved by 1% of the time
where the time goes in v4:
time: 159 us; the launch traced here: 158 us
  Pallas kernels  153 us (96%)
  local copies, waits for them, and re-layouts  5.24 us (3%)
    pallas_call x1, Pallas kernels, per_device(): pl.pallas_call(functools.partial(kernel, n, cap), out_shape=jax.ShapeDtyp...  153 us
    unnamed x3, local copies, waits for them, and re-layouts  5.24 us

profile of v4, /device:TPU:1, one launch (start us, length us, event | category | flops | bytes accessed | tf_op | source)
XLA Modules:
  0.0 158.4 jit_solution(635317648594757041)
XLA Ops:
  0.0 1.5 copy.8.ids_ref
  1.5 1.5 copy.9.gw_ref
  2.9 153.2 %shard_map.73 = bf16[256,2048]{1,0:T(8,128)(2,1)} custom-call(bf16[256,2048]{1,0:T(8,128)(2,1)} %tok_ref.1, f32[1,2048]{1,0:T(1,128)} %bitcast.1, s32[256,2]{1,0:T(8,128)} %copy.8.ids_ref, f32[256,2]{1,0:T(8,128)} %copy.9.gw_ref, bf16[1,2048,1024]{2,1,0:T(8,128)(2,1)} %wg_ref.1, bf16[1,2048,1024]{2,1,0:T(8,128)(2,1)} %wu_ref.1, bf16[1,1024,2048]{2,1,0:T(8,128)(2,1)} %wd_ref.1), custom_call_target="tpu_custom_call" | custom-call | tf_op jit(solution)/shard_map/pallas_call | solution.py:392
  156.1 2.3 %copy.11 = bf16[256,2048]{1,0:T(8,128)(2,1)} copy(bf16[256,2048]{1,0:T(8,128)(2,1)} %shard_map.73) | data formatting | bytes 2097152
